TPU v7x, 32 devices: a whole 2x2x4 slice. The times are simulated.
32 devices in a mesh: fs: 4 (over y, x), tp: 8 (over z, core).
Axes of the slice: x: 2, y: 2, z: 4, core: 2. Of those that a mesh axis runs over, the one named last changes fastest.
Arguments:
- tokens: bfloat16 [4096, 2048], P(('fs', 'tp')), may hold values from -6 to 6
- norm_gain: float32 [2048], replicated, may hold values from 0.1 to 1.9
- gate_weight: bfloat16 [2048, 5632], P('fs', 'tp'), may hold values from -0.125 to 0.125
- up_weight: bfloat16 [2048, 5632], P('fs', 'tp'), may hold values from -0.125 to 0.125
- down_weight: bfloat16 [5632, 2048], P('tp', 'fs'), may hold values from -0.078125 to 0.078125
Outputs:
- mixed: bfloat16 [4096, 2048], P(('fs', 'tp'))
All inputs are finite; a program needn't handle non-finite values.
Results may differ from a plain program's by a relative error of at most 0.0065.
Values may be sent and summed in bfloat16 or wider, within the bound.
A program may use at most 128 MiB of HBM per device.

v0:
```python
import jax
import jax.numpy as jnp
from jax import lax
from jax.sharding import PartitionSpec as P

eps_floor = 0.05


def local(tokens, norm_gain, gate_weight, up_weight, down_weight):
    values = tokens.astype(jnp.float32)
    factor = lax.rsqrt(jnp.mean(values * values, axis=-1, keepdims=True) + eps_floor)
    normed = (values * factor * norm_gain).astype(jnp.bfloat16)
    local_ff = gate_weight.shape[1]
    group = lax.all_gather(normed, "tp", axis=0, tiled=True)
    joined = jnp.concatenate(
        (
            lax.all_gather(gate_weight, "fs", axis=0, tiled=True),
            lax.all_gather(up_weight, "fs", axis=0, tiled=True),
        ),
        axis=1,
    )
    product = jnp.dot(group, joined, preferred_element_type=jnp.float32)
    hidden = (jax.nn.silu(product[:, :local_ff]) * product[:, local_ff:]).astype(jnp.bfloat16)
    down_local = lax.all_gather(down_weight, "fs", axis=1, tiled=True)
    mixed = lax.psum_scatter(
        jnp.dot(hidden, down_local, preferred_element_type=jnp.float32),
        "tp",
        scatter_dimension=0,
        tiled=True,
    )
    return mixed.astype(jnp.bfloat16)


def solution(mesh):
    return jax.shard_map(
        local,
        mesh=mesh,
        in_specs=(P(("fs", "tp"), None), P(), P("fs", "tp"), P("fs", "tp"), P("tp", "fs")),
        out_specs=P(("fs", "tp"), None),
        check_vma=False,
    )
```

profile of v0, /device:TPU:0, one launch (start us, length us, event | category | flops | bytes accessed | tf_op | source)
XLA Modules:
  0.0 296.1 jit_solution(4076748041551358290)
XLA Ops:
  6.5 0.0 all-gather.7.cloned.1.call-start
  6.5 0.7 all-gather.7.cloned.1.call-update
  7.3 0.0 all-gather.9.cloned.1.call-start
  7.3 0.7 all-gather.9.cloned.1.call-update
  8.0 0.0 all-gather.5.cloned.1.call-start
  8.1 1.2 fusion.8
  9.3 2.0 fusion.10
  11.3 0.0 all-gather.5.cloned.1.call-update
  11.3 0.0 all-gather.11.cloned.1.call-start
  11.4 0.5 all-gather.11.cloned.1.call-update
  11.9 0.0 reduce-scatter.2.cloned.1.call-start
  12.0 41.5 %all-gather.7.cloned.1.call-done = bf16[2048,704]{0,1:T(8,128)(2,1)} async-done(((bf16[512,704]{0,1:T(8,128)(2,1)}), bf16[2048,704]{0,1:T(8,128)(2,1)}) %all-gather.7.cloned.1.call-update) | async-done | bytes 2883600 | tf_op jit(solution)/shard_map/all_gather | solution.py:17
  53.5 43.4 %all-gather.9.cloned.1.call-done = bf16[2048,704]{0,1:T(8,128)(2,1)} async-done(((bf16[512,704]{0,1:T(8,128)(2,1)}), bf16[2048,704]{0,1:T(8,128)(2,1)}) %all-gather.9.cloned.1.call-update) | async-done | bytes 2883600 | tf_op jit(solution)/shard_map/all_gather | solution.py:18
  96.9 48.5 %all-gather.5.cloned.1.call-done = bf16[1024,2048]{1,0:T(8,128)(2,1)} async-done(((bf16[128,2048]{1,0:T(8,128)(2,1)}), bf16[1024,2048]{1,0:T(8,128)(2,1)}) %all-gather.5.cloned.1.call-update) | async-done | bytes 4194320 | tf_op jit(solution)/shard_map/all_gather | solution.py:14
  145.4 11.8 %fusion = f32[1024,1408]{1,0:T(8,128)} fusion(bf16[1024,2048]{1,0:T(8,128)(2,1)} %all-gather.5.cloned.1.call-done, bf16[2048,704]{0,1:T(8,128)(2,1)} %all-gather.9.cloned.1.call-done, bf16[2048,704]{0,1:T(8,128)(2,1)} %all-gather.7.cloned.1.call-done), kind=kOutput, calls=%fused_computation | convolution fusion | flops 5917114368 | bytes 15728640 | tf_op jit(solution)/shard_map/dot_general | solution.py:22
  157.2 30.2 %all-gather.11.cloned.1.call-done = bf16[704,2048]{1,0:T(8,128)(2,1)} async-done(((bf16[704,512]{1,0:T(8,128)(2,1)}), bf16[704,2048]{1,0:T(8,128)(2,1)}) %all-gather.11.cloned.1.call-update) | async-done | bytes 2883600 | tf_op jit(solution)/shard_map/all_gather | solution.py:24
  187.4 10.4 %fusion.5 = f32[1024,2048]{1,0:T(8,128)} fusion(bf16[704,2048]{1,0:T(8,128)(2,1)} %all-gather.11.cloned.1.call-done, f32[1024,1408]{1,0:T(8,128)} %fusion), kind=kOutput, calls=%fused_computation.6 | convolution fusion | flops 2957115392 | bytes 17563648 | tf_op jit(solution)/shard_map/dot_general | solution.py:26
  197.8 0.0 reduce-scatter.2.cloned.1.call-update
  197.8 89.7 %reduce-scatter.2.cloned.1.call-done = f32[128,2048]{1,0:T(8,128)} async-done(((f32[1024,2048]{1,0:T(8,128)}), f32[128,2048]{1,0:T(8,128)}) %reduce-scatter.2.cloned.1.call-update) | async-done | bytes 1048592 | tf_op jit(solution)/shard_map/reduce_scatter | solution.py:25
  287.5 2.1 convert_element_type.15
  (1 shorter events, 0.0 us)
Async XLA Ops:
  6.5 46.9 %all-gather.7.cloned.1.call-start = ((), (), s32[]{:S(2)}) async-start(), calls=%async_computation.2 | async-start | bytes 3604480 | tf_op jit(solution)/shard_map/all_gather | solution.py:17
  7.3 89.6 %all-gather.9.cloned.1.call-start = ((), (), s32[]{:S(2)}) async-start(), calls=%async_computation.3 | async-start | bytes 3604480 | tf_op jit(solution)/shard_map/all_gather | solution.py:18
  8.0 137.3 %all-gather.5.cloned.1.call-start = ((), (), s32[]{:S(2)}) async-start(), calls=%async_computation.1 | async-start | bytes 4718592 | tf_op jit(solution)/shard_map/all_gather | solution.py:14
  11.3 176.1 %all-gather.11.cloned.1.call-start = ((), (), s32[]{:S(2)}) async-start(), calls=%async_computation.4 | async-start | bytes 3604480 | tf_op jit(solution)/shard_map/all_gather | solution.py:24
  11.9 275.6 %reduce-scatter.2.cloned.1.call-start = ((), (), s32[]{:S(2)}) async-start(), calls=%async_computation.5 | async-start | bytes 9437184 | tf_op jit(solution)/shard_map/reduce_scatter | solution.py:25
Sparse Core Ops, SparseCore 0:
  9.2 44.2 all-gather.6
  55.3 41.5 all-gather.8
  98.5 46.8 all-gather.4
  147.0 40.3 all-gather.10
  198.0 89.5 reduce-scatter.1
where the time goes:
time: 296 us
  waiting for transfers between devices  255 us (86%)
  matrix products  22.2 us (8%)
  between operations  13.1 us (4%)
  other arithmetic  5.35 us (2%)
    reduce_scatter x1, waiting for transfers between devices, local(): lax.psum_scatter(jnp.dot(hidden, down_local, preferred_element_type=jnp.f...  89.7 us
    all_gather x1, waiting for transfers between devices, local(): group = lax.all_gather(normed, 'tp', axis=0, tiled=True)  48.5 us
    all_gather x1, waiting for transfers between devices, local(): lax.all_gather(up_weight, 'fs', axis=0, tiled=True)  43.4 us
    all_gather x1, waiting for transfers between devices, local(): lax.all_gather(gate_weight, 'fs', axis=0, tiled=True)  41.5 us
    all_gather x1, waiting for transfers between devices, local(): down_local = lax.all_gather(down_weight, 'fs', axis=1, tiled=True)  30.2 us
    dot_general x1, matrix products, local(): product = jnp.dot(group, joined, preferred_element_type=jnp.float32)  11.8 us
    dot_general x1, matrix products, local(): jnp.dot(hidden, down_local, preferred_element_type=jnp.float32)  10.4 us
  transfers between devices with their start and end apart: 5, of which 5 were waited for; matrix products, arithmetic and copies ran while one was open for 5% of the time, Pallas kernels for 0%

commit v1 on v0

v1 whole, which is shorter than its diff:
```python
import functools
import math

import jax
import jax.numpy as jnp
from jax import lax
from jax.experimental import pallas as pl
from jax.experimental.pallas import tpu as pltpu

eps_floor = 0.05
MESH = pl.DeviceIdType.MESH
F32 = jnp.float32
BF16 = jnp.bfloat16


def kernel(Y, X, Z, C, tok, gain, gw, uw, dw, out, nrm, Wg, Wu, Wd, acc_g, acc_u, hid,
           sib_s, sib_r, rs_s, rs_r, out_acc,
           w_send, w_recv, t_send, t_recv, ts_send, ts_recv, p_send, p_recv, q_send, q_recv):
    F = Y * X
    f = lax.axis_index("fs")
    t = lax.axis_index("tp")
    y, x = f // X, f % X
    z, c = t // C, t % C
    rows, D = tok.shape
    K = gw.shape[0]
    H = gw.shape[1]
    N = dw.shape[1]
    tile = 2 if Z % 2 == 0 else 1

    def fs_at(j, i):
        return lax.rem(y + j, Y) * X + lax.rem(x + i, X)

    def tp_at(zz, cc):
        return zz * C + cc

    sib = lax.rem(c + 1, C)

    barrier = pltpu.get_barrier_semaphore()
    peers = [{"fs": fs_at(0, i)} for i in range(1, X)] + [{"fs": fs_at(j, 0)} for j in range(1, Y)]
    peers += [{"tp": tp_at(lax.rem(z + r, Z), c)} for r in range(1, Z)]
    if C > 1:
        peers += [{"tp": tp_at(z, sib)}]
    for peer in peers:
        pl.semaphore_signal(barrier, inc=1, device_id=peer, device_id_type=MESH)

    values = tok[...].astype(F32)
    factor = lax.rsqrt(jnp.mean(values * values, axis=-1, keepdims=True) + eps_floor)
    nrm[c, z] = (values * factor * gain[...]).astype(BF16)
    pl.semaphore_wait(barrier, len(peers))

    mats = ((gw, Wg), (uw, Wu), (dw, Wd))
    w_copies = []

    def half(ref, h):
        n = ref.shape[0] // 2
        return ref.at[pl.ds(h * n, n)]

    def piece(m, h, j, i):
        own, held = mats[m]
        return half(own, h) if (j, i) == (0, 0) else half(held.at[fs_at(j, i)], h)

    def w_copy(m, h, j, i, dj, di):
        k = len(w_copies)
        slot = ((j - dj) % Y) * X + (i - di) % X
        cp = pltpu.make_async_remote_copy(
            src_ref=piece(m, h, j, i), dst_ref=half(mats[m][1].at[fs_at(j, i)], h),
            send_sem=w_send.at[k], recv_sem=w_recv.at[m, h, slot],
            device_id={"fs": fs_at(dj, di)}, device_id_type=MESH)
        cp.start()
        w_copies.append(cp)

    def w_wait(m, h, j, i):
        ref = half(mats[m][1].at[fs_at(j, i)], h)
        pltpu.make_async_copy(ref, ref, w_recv.at[m, h, j * X + i]).wait()

    def phase_one(ms):
        for m in ms:
            for i in range(1, X):
                w_copy(m, 0, 0, 0, 0, i)
            for j in range(1, Y):
                w_copy(m, 1, 0, 0, j, 0)

    def phase_own(ms):
        for m in ms:
            for i in range(1, X):
                w_copy(m, 1, 0, 0, 0, i)
            for j in range(1, Y):
                w_copy(m, 0, 0, 0, j, 0)

    def phase_relay(ms):
        for m in ms:
            for i in range(1, X):
                w_wait(m, 0, 0, i)
                for j in range(1, Y):
                    w_copy(m, 0, 0, i, j, 0)
            for j in range(1, Y):
                w_wait(m, 1, j, 0)
                for i in range(1, X):
                    w_copy(m, 1, j, 0, 0, i)

    def wait_cross(ms):
        for m in ms:
            for i in range(1, X):
                w_wait(m, 1, 0, i)
            for j in range(1, Y):
                w_wait(m, 0, j, 0)

    def wait_diag(ms):
        for m in ms:
            for j in range(1, Y):
                for i in range(1, X):
                    w_wait(m, 0, j, i)
                    w_wait(m, 1, j, i)

    def tok_chain(direction, s):
        src = z - s if direction == 0 else z + s
        dst = z + 1 if direction == 0 else z - 1
        ok = jnp.logical_and(src >= 0, dst < Z) if direction == 0 else jnp.logical_and(src < Z, dst >= 0)
        src, dst = jnp.clip(src, 0, Z - 1), jnp.clip(dst, 0, Z - 1)
        cp = pltpu.make_async_remote_copy(
            src_ref=nrm.at[c, src], dst_ref=nrm.at[c, src],
            send_sem=t_send.at[direction, s], recv_sem=t_recv.at[direction, s],
            device_id={"tp": tp_at(dst, c)}, device_id_type=MESH)
        return cp, ok

    def tok_sib(zz):
        return pltpu.make_async_remote_copy(
            src_ref=nrm.at[c, zz], dst_ref=nrm.at[c, zz],
            send_sem=ts_send.at[zz], recv_sem=ts_recv.at[zz],
            device_id={"tp": tp_at(z, sib)}, device_id_type=MESH)

    def tok_start(s):
        for direction in range(2):
            cp, ok = tok_chain(direction, s)
            pl.when(ok)(cp.start)

    def tok_arrive(s):
        for direction in range(2):
            src = z - s if direction == 0 else z + s
            there = src >= 0 if direction == 0 else src < Z
            src = jnp.clip(src, 0, Z - 1)

            @pl.when(there)
            def _():
                pltpu.make_async_copy(nrm.at[c, src], nrm.at[c, src], t_recv.at[direction, s - 1]).wait()
                if C > 1:
                    tok_sib(src).start()

            if s < Z - 1:
                cp, ok = tok_chain(direction, s)
                pl.when(ok)(cp.start)

    phase_one((0, 1))
    tok_start(0)
    if C > 1:
        tok_sib(z).start()
    phase_own((0, 1))
    if Z > 1:
        tok_arrive(1)
    phase_relay((0, 1))
    for s in range(2, Z):
        tok_arrive(s)
    wait_cross((0, 1))
    phase_one((2,))
    phase_own((2,))
    if C > 1:
        for zz in range(Z):
            ref = nrm.at[sib, zz]
            pltpu.make_async_copy(ref, ref, ts_recv.at[zz]).wait()

    near = [(0, 0)] + [(0, i) for i in range(1, X)] + [(j, 0) for j in range(1, Y)]
    far = [(j, i) for j in range(1, Y) for i in range(1, X)]
    mrows = tile * rows
    per_core = Z // tile

    def products(n, group):
        cc, zt = n // per_core, n % per_core
        g = u = None
        for j, i in group:
            own = (j, i) == (0, 0)
            o = fs_at(j, i)
            a = nrm[cc, pl.ds(zt * tile, tile), :, pl.ds(pl.multiple_of(o * K, K), K)].reshape(mrows, K)
            wg = gw[...] if own else Wg[o]
            wu = uw[...] if own else Wu[o]
            pg = jnp.dot(a, wg, preferred_element_type=F32)
            pu = jnp.dot(a, wu, preferred_element_type=F32)
            g, u = (pg, pu) if g is None else (g + pg, u + pu)
        return g, u

    @pl.loop(0, C * per_core)
    def _(n):
        g, u = products(n, near)
        acc_g[n] = g
        acc_u[n] = u

    wait_diag((0, 1))

    @pl.loop(0, C * per_core)
    def _(n):
        g, u = products(n, far)
        g, u = g + acc_g[n], u + acc_u[n]
        hid[n // per_core, pl.ds((n % per_core) * tile, tile)] = (
            (jax.nn.silu(g) * u).astype(BF16).reshape(tile, rows, H))

    rs_copies = []

    def down_chunk(q, j, i):
        own = (j, i) == (0, 0)
        o = fs_at(j, i)
        cols = pl.ds(pl.multiple_of(o * N, N), N)
        w = (lambda: dw[...]) if own else (lambda: Wd[o])
        if C > 1:
            sib_s[q] = jnp.dot(hid[sib].reshape(Z * rows, H), w(),
                               preferred_element_type=F32).astype(BF16).reshape(Z, rows, N)
            cp = pltpu.make_async_remote_copy(
                src_ref=sib_s.at[q], dst_ref=sib_r.at[q], send_sem=p_send.at[q], recv_sem=p_recv.at[q],
                device_id={"tp": tp_at(z, sib)}, device_id_type=MESH)
            cp.start()
        for r in list(range(1, Z)) + [0]:
            zz = lax.rem(z + r, Z)
            part = jnp.dot(hid[c, zz], w(), preferred_element_type=F32)
            if r == 1 or Z == 1:
                if C > 1:
                    cp.wait_recv()
            if C > 1:
                part = part + sib_r[q, zz].astype(F32)
            if r == 0:
                out_acc[:, cols] = part
            else:
                rs_s[q, r - 1] = part.astype(BF16)
                pltpu.make_async_remote_copy(
                    src_ref=rs_s.at[q, r - 1], dst_ref=rs_r.at[q, r - 1],
                    send_sem=q_send.at[q], recv_sem=q_recv.at[q],
                    device_id={"tp": tp_at(zz, c)}, device_id_type=MESH).start()
        if C > 1:
            rs_copies.append(cp)

    down_chunk(0, 0, 0)
    phase_relay((2,))
    wait_cross((2,))
    q = 1
    for j, i in near[1:]:
        down_chunk(q, j, i)
        q += 1
    wait_diag((2,))
    for j, i in far:
        down_chunk(q, j, i)
        q += 1

    for q, (j, i) in enumerate(near + far):
        cols = pl.ds(pl.multiple_of(fs_at(j, i) * N, N), N)
        total = out_acc[:, cols]
        if Z > 1:
            pltpu.make_async_copy(rs_r.at[q], rs_r.at[q], q_recv.at[q]).wait()
            for r in range(Z - 1):
                total = total + rs_r[q, r].astype(F32)
        out[:, cols] = total.astype(BF16)

    for cp in w_copies:
        cp.wait_send()
    for s in range(Z - 1):
        for direction in range(2):
            cp, ok = tok_chain(direction, s)
            pl.when(ok)(cp.wait_send)
    if C > 1:
        for zz in range(Z):
            tok_sib(zz).wait_send()
        for cp in rs_copies:
            cp.wait_send()
    if Z > 1:
        for q in range(F):
            pltpu.make_async_copy(rs_s.at[q], rs_s.at[q], q_send.at[q]).wait()


def local(sizes, tokens, norm_gain, gate_weight, up_weight, down_weight):
    Y, X, Z, C = sizes
    F = Y * X
    rows, D = tokens.shape
    K, H = gate_weight.shape
    N = down_weight.shape[1]
    tile = 2 if Z % 2 == 0 else 1
    n_w = 3 * ((X - 1) + (Y - 1) * X + (Y - 1) + (X - 1) * Y)
    vmem = pl.BlockSpec(memory_space=pltpu.VMEM)
    dma = pltpu.SemaphoreType.DMA
    hops = max(Z - 1, 1)
    return pl.pallas_call(
        functools.partial(kernel, Y, X, Z, C),
        out_shape=jax.ShapeDtypeStruct((rows, D), BF16),
        in_specs=[vmem] * 5,
        out_specs=vmem,
        scratch_shapes=[
            pltpu.VMEM((C, Z, rows, D), BF16),
            pltpu.VMEM((F, K, H), BF16),
            pltpu.VMEM((F, K, H), BF16),
            pltpu.VMEM((F, H, N), BF16),
            pltpu.VMEM((C * Z // tile, tile * rows, H), F32),
            pltpu.VMEM((C * Z // tile, tile * rows, H), F32),
            pltpu.VMEM((C, Z, rows, H), BF16),
            pltpu.VMEM((F, Z, rows, N), BF16),
            pltpu.VMEM((F, Z, rows, N), BF16),
            pltpu.VMEM((F, hops, rows, N), BF16),
            pltpu.VMEM((F, hops, rows, N), BF16),
            pltpu.VMEM((rows, D), F32),
            dma((max(n_w, 1),)), dma((3, 2, F)),
            dma((2, Z)), dma((2, Z)), dma((Z,)), dma((Z,)),
            dma((F,)), dma((F,)), dma((F,)), dma((F,)),
        ],
        compiler_params=pltpu.CompilerParams(
            collective_id=0, has_side_effects=True, vmem_limit_bytes=60 * 1024 * 1024),
    )(tokens, norm_gain.reshape(1, D), gate_weight, up_weight, down_weight)


def solution(mesh):
    fs, tp = mesh.shape["fs"], mesh.shape["tp"]
    X = max(n for n in range(1, math.isqrt(fs) + 1) if fs % n == 0)
    C = 2 if tp % 2 == 0 else 1
    from jax.sharding import PartitionSpec as P
    return jax.shard_map(
        functools.partial(local, (fs // X, X, tp // C, C)),
        mesh=mesh,
        in_specs=(P(("fs", "tp"), None), P(), P("fs", "tp"), P("fs", "tp"), P("tp", "fs")),
        out_specs=P(("fs", "tp"), None),
        check_vma=False,
    )
```

time: 296 us -> 118 us (0.40)
  waiting for transfers between devices: 255 us -> 0 us
  Pallas kernels: 0 us -> 111 us
  matrix products: 22.2 us -> 0 us
  between operations: 13.1 us -> 0.01 us
  local copies, waits for them, and re-layouts: 0 us -> 5.4 us
  other arithmetic: 5.35 us -> 0 us
    all_gather x4 -> x0, waiting for transfers between devices: 164 us -> none  [the longest x1 48.5 us: local(): group = lax.all_gather(normed, 'tp', axis=0, tiled=True)]
    pallas_call x0 -> x1, Pallas kernels: none -> 111 us  [local(): pl.pallas_call(functools.partial(kernel, Y, X, Z, C), out_shape=jax.Shape...]
    reduce_scatter x1 -> x0, waiting for transfers between devices: 89.7 us -> none  [local(): lax.psum_scatter(jnp.dot(hidden, down_local, preferred_element_type=jnp.f...]
    dot_general x2 -> x0, matrix products: 22.2 us -> none  [the longest x1 11.8 us: local(): product = jnp.dot(group, joined, preferred_element_type=jnp.float32)]
    unnamed x0 -> x5, local copies, waits for them, and re-layouts: none -> 5.4 us
    convert_element_type x2 -> x0, other arithmetic: 4.11 us -> none  [the longest x1 2.08 us: local(): return mixed.astype(jnp.bfloat16)]
  transfers between devices with their start and end apart: 5 -> 0, of which waited for: 5 -> 0; matrix products, arithmetic and copies ran while one was open for 5% -> 0% of each run, Pallas kernels for 0% -> 0%
where the time goes in v1:
time: 118 us; the launch traced here: 116 us
  Pallas kernels  111 us (94%)
  local copies, waits for them, and re-layouts  5.4 us (5%)
    pallas_call x1, Pallas kernels, local(): pl.pallas_call(functools.partial(kernel, Y, X, Z, C), out_shape=jax.Shape...  111 us
    unnamed x5, local copies, waits for them, and re-layouts  5.4 us

profile of v1, /device:TPU:0, one launch (start us, length us, event | category | flops | bytes accessed | tf_op | source)
XLA Modules:
  0.0 116.4 jit_solution(286646206229230477)
XLA Ops:
  0.0 0.0 copy-start
  0.0 2.3 %copy.6.gw = bf16[512,704]{1,0:T(8,128)(2,1)} copy(bf16[512,704]{0,1:T(8,128)(2,1)} %param.7) | data formatting | bytes 1441792 | tf_op args[2]
  2.3 0.0 copy-done
  2.3 1.2 %copy.7.uw = bf16[512,704]{1,0:T(8,128)(2,1)} copy(bf16[512,704]{0,1:T(8,128)(2,1)S(1)} %copy-done) | data formatting | bytes 1441792 | tf_op args[3]
  3.5 111.0 %shard_map.55 = bf16[128,2048]{1,0:T(8,128)(2,1)} custom-call(bf16[128,2048]{1,0:T(8,128)(2,1)} %tok.1, f32[1,2048]{1,0:T(1,128)} %bitcast.1, bf16[512,704]{1,0:T(8,128)(2,1)} %copy.6.gw, bf16[512,704]{1,0:T(8,128)(2,1)} %copy.7.uw, bf16[704,512]{1,0:T(8,128)(2,1)} %dw.1), custom_call_target="tpu_custom_call" | custom-call | tf_op jit(solution)/shard_map/pallas_call | solution.py:286
  114.5 1.9 %copy.9 = bf16[128,2048]{1,0:T(8,128)(2,1)} copy(bf16[128,2048]{1,0:T(8,128)(2,1)} %shard_map.55) | data formatting | bytes 1048576
Async XLA Ops:
  0.0 2.3 %copy-start = (bf16[512,704]{0,1:T(8,128)(2,1)S(1)}, bf16[512,704]{0,1:T(8,128)(2,1)}, u32[]{:S(2)}) copy-start(bf16[512,704]{0,1:T(8,128)(2,1)} %param.8) | copy-start | bytes 2162692

commit v2 on v1

--- a/solution.py
+++ b/solution.py
@@ -14,7 +14,7 @@
 
 
 def kernel(Y, X, Z, C, tok, gain, gw, uw, dw, out, nrm, Wg, Wu, Wd, acc_g, acc_u, hid,
-           sib_s, sib_r, rs_s, rs_r, out_acc,
+           sib_s, sib_r, rs_s, rs_r, part, w_local,
            w_send, w_recv, t_send, t_recv, ts_send, ts_recv, p_send, p_recv, q_send, q_recv):
     F = Y * X
     f = lax.axis_index("fs")
@@ -22,8 +22,7 @@
     y, x = f // X, f % X
     z, c = t // C, t % C
     rows, D = tok.shape
-    K = gw.shape[0]
-    H = gw.shape[1]
+    H, K = gw.shape
     N = dw.shape[1]
     tile = 2 if Z % 2 == 0 else 1
 
@@ -37,18 +36,30 @@
 
     barrier = pltpu.get_barrier_semaphore()
     peers = [{"fs": fs_at(0, i)} for i in range(1, X)] + [{"fs": fs_at(j, 0)} for j in range(1, Y)]
-    peers += [{"tp": tp_at(lax.rem(z + r, Z), c)} for r in range(1, Z)]
     if C > 1:
         peers += [{"tp": tp_at(z, sib)}]
+
+    def greet(peer):
+        pl.semaphore_signal(barrier, inc=1, device_id=peer, device_id_type=MESH)
+
     for peer in peers:
-        pl.semaphore_signal(barrier, inc=1, device_id=peer, device_id_type=MESH)
+        greet(peer)
+    below, above = jnp.maximum(z - 1, 0), jnp.minimum(z + 1, Z - 1)
+    pl.when(z > 0)(lambda: greet({"tp": tp_at(below, c)}))
+    pl.when(z < Z - 1)(lambda: greet({"tp": tp_at(above, c)}))
+
+    mats = ((gw, Wg), (uw, Wu), (dw, Wd))
+    own_copies = [pltpu.make_async_copy(ref, held.at[f], w_local.at[m]) for m, (ref, held) in enumerate(mats)]
+    for cp in own_copies:
+        cp.start()
 
     values = tok[...].astype(F32)
     factor = lax.rsqrt(jnp.mean(values * values, axis=-1, keepdims=True) + eps_floor)
     nrm[c, z] = (values * factor * gain[...]).astype(BF16)
-    pl.semaphore_wait(barrier, len(peers))
-
-    mats = ((gw, Wg), (uw, Wu), (dw, Wd))
+    pl.semaphore_wait(barrier, len(peers) + (z > 0).astype(jnp.int32) + (z < Z - 1).astype(jnp.int32))
+    for cp in own_copies:
+        cp.wait()
+
     w_copies = []
 
     def half(ref, h):
@@ -56,8 +67,7 @@
         return ref.at[pl.ds(h * n, n)]
 
     def piece(m, h, j, i):
-        own, held = mats[m]
-        return half(own, h) if (j, i) == (0, 0) else half(held.at[fs_at(j, i)], h)
+        return half(mats[m][1].at[fs_at(j, i)], h)
 
     def w_copy(m, h, j, i, dj, di):
         k = len(w_copies)
@@ -177,13 +187,10 @@
         cc, zt = n // per_core, n % per_core
         g = u = None
         for j, i in group:
-            own = (j, i) == (0, 0)
             o = fs_at(j, i)
             a = nrm[cc, pl.ds(zt * tile, tile), :, pl.ds(pl.multiple_of(o * K, K), K)].reshape(mrows, K)
-            wg = gw[...] if own else Wg[o]
-            wu = uw[...] if own else Wu[o]
-            pg = jnp.dot(a, wg, preferred_element_type=F32)
-            pu = jnp.dot(a, wu, preferred_element_type=F32)
+            pg = lax.dot_general(a, Wg[o], (((1,), (1,)), ((), ())), preferred_element_type=F32)
+            pu = lax.dot_general(a, Wu[o], (((1,), (1,)), ((), ())), preferred_element_type=F32)
             g, u = (pg, pu) if g is None else (g + pg, u + pu)
         return g, u
 
@@ -202,59 +209,80 @@
         hid[n // per_core, pl.ds((n % per_core) * tile, tile)] = (
             (jax.nn.silu(g) * u).astype(BF16).reshape(tile, rows, H))
 
-    rs_copies = []
+    sib_copies = []
+
+    def sum_copy(q, direction, d):
+        to = above if direction == 0 else below
+        return pltpu.make_async_remote_copy(
+            src_ref=rs_s.at[q, d], dst_ref=rs_r.at[q, direction, d],
+            send_sem=q_send.at[q, d], recv_sem=q_recv.at[q, direction, d],
+            device_id={"tp": tp_at(to, c)}, device_id_type=MESH)
+
+    def sum_wait(q, direction, d):
+        ref = rs_r.at[q, direction, d]
+        pltpu.make_async_copy(ref, ref, q_recv.at[q, direction, d]).wait()
 
     def down_chunk(q, j, i):
-        own = (j, i) == (0, 0)
         o = fs_at(j, i)
-        cols = pl.ds(pl.multiple_of(o * N, N), N)
-        w = (lambda: dw[...]) if own else (lambda: Wd[o])
         if C > 1:
-            sib_s[q] = jnp.dot(hid[sib].reshape(Z * rows, H), w(),
+            sib_s[q] = jnp.dot(hid[sib].reshape(Z * rows, H), Wd[o],
                                preferred_element_type=F32).astype(BF16).reshape(Z, rows, N)
             cp = pltpu.make_async_remote_copy(
                 src_ref=sib_s.at[q], dst_ref=sib_r.at[q], send_sem=p_send.at[q], recv_sem=p_recv.at[q],
                 device_id={"tp": tp_at(z, sib)}, device_id_type=MESH)
             cp.start()
-        for r in list(range(1, Z)) + [0]:
-            zz = lax.rem(z + r, Z)
-            part = jnp.dot(hid[c, zz], w(), preferred_element_type=F32)
-            if r == 1 or Z == 1:
-                if C > 1:
-                    cp.wait_recv()
-            if C > 1:
-                part = part + sib_r[q, zz].astype(F32)
-            if r == 0:
-                out_acc[:, cols] = part
-            else:
-                rs_s[q, r - 1] = part.astype(BF16)
-                pltpu.make_async_remote_copy(
-                    src_ref=rs_s.at[q, r - 1], dst_ref=rs_r.at[q, r - 1],
-                    send_sem=q_send.at[q], recv_sem=q_recv.at[q],
-                    device_id={"tp": tp_at(zz, c)}, device_id_type=MESH).start()
+            sib_copies.append(cp)
+        part[q] = jnp.dot(hid[c].reshape(Z * rows, H), Wd[o],
+                          preferred_element_type=F32).reshape(Z, rows, N)
         if C > 1:
-            rs_copies.append(cp)
-
+            cp.wait_recv()
+
+            @pl.loop(0, Z)
+            def _(d):
+                part[q, d] = part[q, d] + sib_r[q, d].astype(F32)
+
+        for direction, first, order in ((0, z == 0, range(Z - 1, 0, -1)), (1, z == Z - 1, range(Z - 1))):
+            @pl.when(first)
+            def _():
+                for d in order:
+                    rs_s[q, d] = part[q, d].astype(BF16)
+                    sum_copy(q, direction, d).start()
+
+    def sum_relay(q):
+        for k in range(Z - 1):
+            for direction, d in ((0, Z - 1 - k), (1, k)):
+                ok = jnp.logical_and(z > 0, z < d) if direction == 0 else jnp.logical_and(z < Z - 1, z > d)
+
+                @pl.when(ok)
+                def _():
+                    sum_wait(q, direction, d)
+                    rs_s[q, d] = (part[q, d] + rs_r[q, direction, d].astype(F32)).astype(BF16)
+                    sum_copy(q, direction, d).start()
+
+    def sum_end(q, j, i):
+        for direction, there in ((0, z > 0), (1, z < Z - 1)):
+            @pl.when(there)
+            def _():
+                sum_wait(q, direction, z)
+                part[q, z] = part[q, z] + rs_r[q, direction, z].astype(F32)
+
+        out[:, pl.ds(pl.multiple_of(fs_at(j, i) * N, N), N)] = part[q, z].astype(BF16)
+
+    order = near + far
     down_chunk(0, 0, 0)
     phase_relay((2,))
+    sum_relay(0)
     wait_cross((2,))
-    q = 1
-    for j, i in near[1:]:
-        down_chunk(q, j, i)
-        q += 1
-    wait_diag((2,))
-    for j, i in far:
-        down_chunk(q, j, i)
-        q += 1
-
-    for q, (j, i) in enumerate(near + far):
-        cols = pl.ds(pl.multiple_of(fs_at(j, i) * N, N), N)
-        total = out_acc[:, cols]
-        if Z > 1:
-            pltpu.make_async_copy(rs_r.at[q], rs_r.at[q], q_recv.at[q]).wait()
-            for r in range(Z - 1):
-                total = total + rs_r[q, r].astype(F32)
-        out[:, cols] = total.astype(BF16)
+    for q in range(1, len(order)):
+        if q == len(near):
+            wait_diag((2,))
+        down_chunk(q, *order[q])
+        if q > 1:
+            sum_relay(q - 1)
+    if len(order) > 1:
+        sum_relay(len(order) - 1)
+    for q in range(len(order)):
+        sum_end(q, *order[q])
 
     for cp in w_copies:
         cp.wait_send()
@@ -265,45 +293,47 @@
     if C > 1:
         for zz in range(Z):
             tok_sib(zz).wait_send()
-        for cp in rs_copies:
+        for cp in sib_copies:
             cp.wait_send()
-    if Z > 1:
-        for q in range(F):
-            pltpu.make_async_copy(rs_s.at[q], rs_s.at[q], q_send.at[q]).wait()
+    for q in range(F):
+        for d in range(Z):
+            pl.when(z != d)(sum_copy(q, 0, d).wait_send)
 
 
 def local(sizes, tokens, norm_gain, gate_weight, up_weight, down_weight):
     Y, X, Z, C = sizes
     F = Y * X
     rows, D = tokens.shape
-    K, H = gate_weight.shape
+    gate_weight, up_weight = gate_weight.T, up_weight.T
+    H, K = gate_weight.shape
     N = down_weight.shape[1]
     tile = 2 if Z % 2 == 0 else 1
     n_w = 3 * ((X - 1) + (Y - 1) * X + (Y - 1) + (X - 1) * Y)
     vmem = pl.BlockSpec(memory_space=pltpu.VMEM)
     dma = pltpu.SemaphoreType.DMA
-    hops = max(Z - 1, 1)
+    hbm = pl.BlockSpec(memory_space=pl.ANY)
     return pl.pallas_call(
         functools.partial(kernel, Y, X, Z, C),
         out_shape=jax.ShapeDtypeStruct((rows, D), BF16),
-        in_specs=[vmem] * 5,
+        in_specs=[vmem] * 2 + [hbm] * 3,
         out_specs=vmem,
         scratch_shapes=[
             pltpu.VMEM((C, Z, rows, D), BF16),
-            pltpu.VMEM((F, K, H), BF16),
-            pltpu.VMEM((F, K, H), BF16),
+            pltpu.VMEM((F, H, K), BF16),
+            pltpu.VMEM((F, H, K), BF16),
             pltpu.VMEM((F, H, N), BF16),
             pltpu.VMEM((C * Z // tile, tile * rows, H), F32),
             pltpu.VMEM((C * Z // tile, tile * rows, H), F32),
             pltpu.VMEM((C, Z, rows, H), BF16),
             pltpu.VMEM((F, Z, rows, N), BF16),
             pltpu.VMEM((F, Z, rows, N), BF16),
-            pltpu.VMEM((F, hops, rows, N), BF16),
-            pltpu.VMEM((F, hops, rows, N), BF16),
-            pltpu.VMEM((rows, D), F32),
+            pltpu.VMEM((F, Z, rows, N), BF16),
+            pltpu.VMEM((F, 2, Z, rows, N), BF16),
+            pltpu.VMEM((F, Z, rows, N), F32),
+            dma((3,)),
             dma((max(n_w, 1),)), dma((3, 2, F)),
             dma((2, Z)), dma((2, Z)), dma((Z,)), dma((Z,)),
-            dma((F,)), dma((F,)), dma((F,)), dma((F,)),
+            dma((F,)), dma((F,)), dma((F, Z)), dma((F, 2, Z)),
         ],
         compiler_params=pltpu.CompilerParams(
             collective_id=0, has_side_effects=True, vmem_limit_bytes=60 * 1024 * 1024),

time: 118 us -> 120 us (1.017)
  Pallas kernels: 111 us -> 118 us
  local copies, waits for them, and re-layouts: 5.4 us -> 1.88 us
    pallas_call x1, Pallas kernels: 111 us -> 118 us  [local(): pl.pallas_call(functools.partial(kernel, Y, X, Z, C), out_shape=jax.Shape...]
    unnamed x5 -> x1, local copies, waits for them, and re-layouts: 5.4 us -> 1.88 us
where the time goes in v2:
time: 120 us
  Pallas kernels  118 us (98%)
  local copies, waits for them, and re-layouts  1.88 us (2%)
    pallas_call x1, Pallas kernels, local(): pl.pallas_call(functools.partial(kernel, Y, X, Z, C), out_shape=jax.Shape...  118 us

profile of v2, /device:TPU:0, one launch (start us, length us, event | category | flops | bytes accessed | tf_op | source)
XLA Modules:
  0.0 119.6 jit_solution(10047875863205663864)
XLA Ops:
  0.0 117.7 %shard_map.55 = bf16[128,2048]{1,0:T(8,128)(2,1)} custom-call(bf16[128,2048]{1,0:T(8,128)(2,1)} %tok.1, f32[1,2048]{1,0:T(1,128)} %bitcast.5, bf16[704,512]{1,0:T(8,128)(2,1)} %bitcast.3, bf16[704,512]{1,0:T(8,128)(2,1)} %bitcast.4, bf16[704,512]{1,0:T(8,128)(2,1)} %dw.1), custom_call_target="tpu_custom_call" | custom-call | tf_op jit(solution)/shard_map/pallas_call | solution.py:315
  117.7 1.9 %copy.7 = bf16[128,2048]{1,0:T(8,128)(2,1)} copy(bf16[128,2048]{1,0:T(8,128)(2,1)} %shard_map.55) | data formatting | bytes 1048576

commit v3 on v2

--- a/solution.py
+++ b/solution.py
@@ -13,7 +13,7 @@
 BF16 = jnp.bfloat16
 
 
-def kernel(Y, X, Z, C, tok, gain, gw, uw, dw, out, nrm, Wg, Wu, Wd, acc_g, acc_u, hid,
+def kernel(Y, X, Z, C, cuts, tok, gain, gw, uw, dw, out, nrm, Wg, Wu, Wd, acc_g, acc_u, hid,
            sib_s, sib_r, rs_s, rs_r, part, w_local,
            w_send, w_recv, t_send, t_recv, ts_send, ts_recv, p_send, p_recv, q_send, q_recv):
     F = Y * X
@@ -23,7 +23,7 @@
     z, c = t // C, t % C
     rows, D = tok.shape
     H, K = gw.shape
-    N = dw.shape[1]
+    N = dw.shape[1] // cuts
     tile = 2 if Z % 2 == 0 else 1
 
     def fs_at(j, i):
@@ -62,25 +62,25 @@
 
     w_copies = []
 
-    def half(ref, h):
-        n = ref.shape[0] // 2
-        return ref.at[pl.ds(h * n, n)]
-
     def piece(m, h, j, i):
-        return half(mats[m][1].at[fs_at(j, i)], h)
+        held = mats[m][1].at[fs_at(j, i)]
+        if m == 2 and cuts == 2:
+            return held.at[:, pl.ds(h * N, N)]
+        n = held.shape[0] // 2
+        return held.at[pl.ds(h * n, n)]
 
     def w_copy(m, h, j, i, dj, di):
         k = len(w_copies)
         slot = ((j - dj) % Y) * X + (i - di) % X
         cp = pltpu.make_async_remote_copy(
-            src_ref=piece(m, h, j, i), dst_ref=half(mats[m][1].at[fs_at(j, i)], h),
+            src_ref=piece(m, h, j, i), dst_ref=piece(m, h, j, i),
             send_sem=w_send.at[k], recv_sem=w_recv.at[m, h, slot],
             device_id={"fs": fs_at(dj, di)}, device_id_type=MESH)
         cp.start()
         w_copies.append(cp)
 
     def w_wait(m, h, j, i):
-        ref = half(mats[m][1].at[fs_at(j, i)], h)
+        ref = piece(m, h, j, i)
         pltpu.make_async_copy(ref, ref, w_recv.at[m, h, j * X + i]).wait()
 
     def phase_one(ms):
@@ -222,67 +222,103 @@
         ref = rs_r.at[q, direction, d]
         pltpu.make_async_copy(ref, ref, q_recv.at[q, direction, d]).wait()
 
-    def down_chunk(q, j, i):
-        o = fs_at(j, i)
+    units = []
+
+    def down(new):
+        qs = list(range(len(units), len(units) + len(new)))
+        units.extend(new)
+
+        def weight(q):
+            j, i, h = units[q]
+            return Wd[fs_at(j, i), :, h * N:(h + 1) * N]
+
+        copies = []
         if C > 1:
-            sib_s[q] = jnp.dot(hid[sib].reshape(Z * rows, H), Wd[o],
-                               preferred_element_type=F32).astype(BF16).reshape(Z, rows, N)
-            cp = pltpu.make_async_remote_copy(
-                src_ref=sib_s.at[q], dst_ref=sib_r.at[q], send_sem=p_send.at[q], recv_sem=p_recv.at[q],
-                device_id={"tp": tp_at(z, sib)}, device_id_type=MESH)
-            cp.start()
-            sib_copies.append(cp)
-        part[q] = jnp.dot(hid[c].reshape(Z * rows, H), Wd[o],
-                          preferred_element_type=F32).reshape(Z, rows, N)
-        if C > 1:
+            for q in qs:
+                sib_s[q] = jnp.dot(hid[sib].reshape(Z * rows, H), weight(q),
+                                   preferred_element_type=F32).astype(BF16).reshape(Z, rows, N)
+                cp = pltpu.make_async_remote_copy(
+                    src_ref=sib_s.at[q], dst_ref=sib_r.at[q], send_sem=p_send.at[q], recv_sem=p_recv.at[q],
+                    device_id={"tp": tp_at(z, sib)}, device_id_type=MESH)
+                cp.start()
+                copies.append(cp)
+        for q in qs:
+            part[q] = jnp.dot(hid[c].reshape(Z * rows, H), weight(q),
+                              preferred_element_type=F32).reshape(Z, rows, N)
+        for q, cp in zip(qs, copies):
             cp.wait_recv()
 
             @pl.loop(0, Z)
             def _(d):
                 part[q, d] = part[q, d] + sib_r[q, d].astype(F32)
+        sib_copies.extend(copies)
 
         for direction, first, order in ((0, z == 0, range(Z - 1, 0, -1)), (1, z == Z - 1, range(Z - 1))):
             @pl.when(first)
             def _():
                 for d in order:
-                    rs_s[q, d] = part[q, d].astype(BF16)
-                    sum_copy(q, direction, d).start()
-
-    def sum_relay(q):
-        for k in range(Z - 1):
-            for direction, d in ((0, Z - 1 - k), (1, k)):
-                ok = jnp.logical_and(z > 0, z < d) if direction == 0 else jnp.logical_and(z < Z - 1, z > d)
-
-                @pl.when(ok)
-                def _():
-                    sum_wait(q, direction, d)
-                    rs_s[q, d] = (part[q, d] + rs_r[q, direction, d].astype(F32)).astype(BF16)
-                    sum_copy(q, direction, d).start()
-
-    def sum_end(q, j, i):
+                    for q in qs:
+                        rs_s[q, d] = part[q, d].astype(BF16)
+                        sum_copy(q, direction, d).start()
+        return qs
+
+    low = 2 * z < Z
+
+    def sum_step(q, direction, d, ok):
+        @pl.when(ok)
+        def _():
+            sum_wait(q, direction, d)
+            rs_s[q, d] = (part[q, d] + rs_r[q, direction, d].astype(F32)).astype(BF16)
+            sum_copy(q, direction, d).start()
+
+    def sum_near(qs):
+        for d in range(Z - 1, 0, -1):
+            for q in qs:
+                sum_step(q, 0, d, jnp.logical_and(jnp.logical_and(z > 0, z < d), low))
+        for d in range(Z - 1):
+            for q in qs:
+                sum_step(q, 1, d, jnp.logical_and(jnp.logical_and(z < Z - 1, z > d), jnp.logical_not(low)))
+
+    def sum_far(qs):
+        for d in range(Z - 1, 0, -1):
+            for q in qs:
+                sum_step(q, 0, d, jnp.logical_and(z < d, jnp.logical_not(low)))
+        for d in range(Z - 1):
+            for q in qs:
+                sum_step(q, 1, d, jnp.logical_and(z > d, low))
+
+    def sum_end(q):
+        j, i, h = units[q]
         for direction, there in ((0, z > 0), (1, z < Z - 1)):
             @pl.when(there)
             def _():
                 sum_wait(q, direction, z)
                 part[q, z] = part[q, z] + rs_r[q, direction, z].astype(F32)
 
-        out[:, pl.ds(pl.multiple_of(fs_at(j, i) * N, N), N)] = part[q, z].astype(BF16)
-
-    order = near + far
-    down_chunk(0, 0, 0)
+        out[:, pl.ds(pl.multiple_of((fs_at(j, i) * cuts + h) * N, N), N)] = part[q, z].astype(BF16)
+
+    in_row = [(0, i) for i in range(1, X)]
+    in_col = [(j, 0) for j in range(1, Y)]
+    both = range(cuts)
+    early = [(j, i, 0) for j, i in in_row] + [(j, i, 1) for j, i in in_col] if cuts == 2 else []
+    mid = [(j, i, h) for h in both for j, i in in_row + in_col if (j, i, h) not in early]
+    qa = down([(0, 0, h) for h in both])
     phase_relay((2,))
-    sum_relay(0)
+    qb = down(early)
+    sum_near(qa)
     wait_cross((2,))
-    for q in range(1, len(order)):
-        if q == len(near):
-            wait_diag((2,))
-        down_chunk(q, *order[q])
-        if q > 1:
-            sum_relay(q - 1)
-    if len(order) > 1:
-        sum_relay(len(order) - 1)
-    for q in range(len(order)):
-        sum_end(q, *order[q])
+    qc = down(mid)
+    sum_near(qb)
+    sum_far(qa)
+    wait_diag((2,))
+    qd = down([(j, i, h) for j, i in far for h in both])
+    sum_near(qc)
+    sum_far(qb)
+    sum_near(qd)
+    sum_far(qc)
+    sum_far(qd)
+    for q in range(len(units)):
+        sum_end(q)
 
     for cp in w_copies:
         cp.wait_send()
@@ -295,7 +331,7 @@
             tok_sib(zz).wait_send()
         for cp in sib_copies:
             cp.wait_send()
-    for q in range(F):
+    for q in range(len(units)):
         for d in range(Z):
             pl.when(z != d)(sum_copy(q, 0, d).wait_send)
 
@@ -306,14 +342,16 @@
     rows, D = tokens.shape
     gate_weight, up_weight = gate_weight.T, up_weight.T
     H, K = gate_weight.shape
-    N = down_weight.shape[1]
+    cuts = 2 if down_weight.shape[1] % 256 == 0 else 1
+    N = down_weight.shape[1] // cuts
+    U = F * cuts
     tile = 2 if Z % 2 == 0 else 1
     n_w = 3 * ((X - 1) + (Y - 1) * X + (Y - 1) + (X - 1) * Y)
     vmem = pl.BlockSpec(memory_space=pltpu.VMEM)
     dma = pltpu.SemaphoreType.DMA
     hbm = pl.BlockSpec(memory_space=pl.ANY)
     return pl.pallas_call(
-        functools.partial(kernel, Y, X, Z, C),
+        functools.partial(kernel, Y, X, Z, C, cuts),
         out_shape=jax.ShapeDtypeStruct((rows, D), BF16),
         in_specs=[vmem] * 2 + [hbm] * 3,
         out_specs=vmem,
@@ -321,19 +359,19 @@
             pltpu.VMEM((C, Z, rows, D), BF16),
             pltpu.VMEM((F, H, K), BF16),
             pltpu.VMEM((F, H, K), BF16),
-            pltpu.VMEM((F, H, N), BF16),
+            pltpu.VMEM((F, H, N * cuts), BF16),
             pltpu.VMEM((C * Z // tile, tile * rows, H), F32),
             pltpu.VMEM((C * Z // tile, tile * rows, H), F32),
             pltpu.VMEM((C, Z, rows, H), BF16),
-            pltpu.VMEM((F, Z, rows, N), BF16),
-            pltpu.VMEM((F, Z, rows, N), BF16),
-            pltpu.VMEM((F, Z, rows, N), BF16),
-            pltpu.VMEM((F, 2, Z, rows, N), BF16),
-            pltpu.VMEM((F, Z, rows, N), F32),
+            pltpu.VMEM((U, Z, rows, N), BF16),
+            pltpu.VMEM((U, Z, rows, N), BF16),
+            pltpu.VMEM((U, Z, rows, N), BF16),
+            pltpu.VMEM((U, 2, Z, rows, N), BF16),
+            pltpu.VMEM((U, Z, rows, N), F32),
             dma((3,)),
             dma((max(n_w, 1),)), dma((3, 2, F)),
             dma((2, Z)), dma((2, Z)), dma((Z,)), dma((Z,)),
-            dma((F,)), dma((F,)), dma((F, Z)), dma((F, 2, Z)),
+            dma((U,)), dma((U,)), dma((U, Z)), dma((U, 2, Z)),
         ],
         compiler_params=pltpu.CompilerParams(
             collective_id=0, has_side_effects=True, vmem_limit_bytes=60 * 1024 * 1024),

time: 120 us -> 104 us (0.87)
  Pallas kernels: 118 us -> 102 us
    pallas_call x1, Pallas kernels: 118 us -> 102 us  [local(): pl.pallas_call(functools.partial(kernel, Y, X, Z, C, cuts), out_shape=jax...]
where the time goes in v3:
time: 104 us; the launch traced here: 103 us
  Pallas kernels  102 us (98%)
  local copies, waits for them, and re-layouts  1.88 us (2%)
    pallas_call x1, Pallas kernels, local(): pl.pallas_call(functools.partial(kernel, Y, X, Z, C, cuts), out_shape=jax...  102 us

profile of v3, /device:TPU:0, one launch (start us, length us, event | category | flops | bytes accessed | tf_op | source)
XLA Modules:
  0.0 103.5 jit_solution(11906860742757324096)
XLA Ops:
  0.0 101.6 %shard_map.55 = bf16[128,2048]{1,0:T(8,128)(2,1)} custom-call(bf16[128,2048]{1,0:T(8,128)(2,1)} %tok.1, f32[1,2048]{1,0:T(1,128)} %bitcast.5, bf16[704,512]{1,0:T(8,128)(2,1)} %bitcast.3, bf16[704,512]{1,0:T(8,128)(2,1)} %bitcast.4, bf16[704,512]{1,0:T(8,128)(2,1)} %dw.1), custom_call_target="tpu_custom_call" | custom-call | tf_op jit(solution)/shard_map/pallas_call | solution.py:353
  101.6 1.9 %copy.7 = bf16[128,2048]{1,0:T(8,128)(2,1)} copy(bf16[128,2048]{1,0:T(8,128)(2,1)} %shard_map.55) | data formatting | bytes 1048576

commit v4 on v3

--- a/solution.py
+++ b/solution.py
@@ -183,31 +183,38 @@
     mrows = tile * rows
     per_core = Z // tile
 
-    def products(n, group):
+    def product(n, held, group):
         cc, zt = n // per_core, n % per_core
-        g = u = None
+        total = None
         for j, i in group:
             o = fs_at(j, i)
             a = nrm[cc, pl.ds(zt * tile, tile), :, pl.ds(pl.multiple_of(o * K, K), K)].reshape(mrows, K)
-            pg = lax.dot_general(a, Wg[o], (((1,), (1,)), ((), ())), preferred_element_type=F32)
-            pu = lax.dot_general(a, Wu[o], (((1,), (1,)), ((), ())), preferred_element_type=F32)
-            g, u = (pg, pu) if g is None else (g + pg, u + pu)
-        return g, u
+            p = lax.dot_general(a, held[o], (((1,), (1,)), ((), ())), preferred_element_type=F32)
+            total = p if total is None else total + p
+        return total
 
     @pl.loop(0, C * per_core)
     def _(n):
-        g, u = products(n, near)
-        acc_g[n] = g
-        acc_u[n] = u
-
-    wait_diag((0, 1))
+        acc_g[n] = product(n, Wg, near)
+        acc_u[n] = product(n, Wu, near)
+
+    wait_diag((0,))
 
     @pl.loop(0, C * per_core)
     def _(n):
-        g, u = products(n, far)
-        g, u = g + acc_g[n], u + acc_u[n]
-        hid[n // per_core, pl.ds((n % per_core) * tile, tile)] = (
-            (jax.nn.silu(g) * u).astype(BF16).reshape(tile, rows, H))
+        g = acc_g[n]
+        if far:
+            g = g + product(n, Wg, far)
+        acc_g[n] = jax.nn.silu(g)
+
+    wait_diag((1,))
+
+    @pl.loop(0, C * per_core)
+    def _(n):
+        u = acc_u[n]
+        if far:
+            u = u + product(n, Wu, far)
+        hid[n // per_core, pl.ds((n % per_core) * tile, tile)] = (acc_g[n] * u).astype(BF16).reshape(tile, rows, H)
 
     sib_copies = []
 
@@ -302,7 +309,7 @@
     both = range(cuts)
     early = [(j, i, 0) for j, i in in_row] + [(j, i, 1) for j, i in in_col] if cuts == 2 else []
     mid = [(j, i, h) for h in both for j, i in in_row + in_col if (j, i, h) not in early]
-    qa = down([(0, 0, h) for h in both])
+    qa = [q for h in both for q in down([(0, 0, h)])]
     phase_relay((2,))
     qb = down(early)
     sum_near(qa)
@@ -314,10 +321,14 @@
     qd = down([(j, i, h) for j, i in far for h in both])
     sum_near(qc)
     sum_far(qb)
+    for q in qa + qb:
+        sum_end(q)
+    sum_far(qc)
     sum_near(qd)
-    sum_far(qc)
+    for q in qc:
+        sum_end(q)
     sum_far(qd)
-    for q in range(len(units)):
+    for q in qd:
         sum_end(q)
 
     for cp in w_copies:
@@ -352,7 +363,7 @@
     hbm = pl.BlockSpec(memory_space=pl.ANY)
     return pl.pallas_call(
         functools.partial(kernel, Y, X, Z, C, cuts),
-        out_shape=jax.ShapeDtypeStruct((rows, D), BF16),
+        out_shape=pltpu.VMEM((rows, D), BF16),
         in_specs=[vmem] * 2 + [hbm] * 3,
         out_specs=vmem,
         scratch_shapes=[

time: 104 us -> 98.4 us (0.946)
  Pallas kernels: 102 us -> 97.4 us
  local copies, waits for them, and re-layouts: 1.88 us -> 0.8 us
    pallas_call x1, Pallas kernels: 102 us -> 97.4 us  [local(): pl.pallas_call(functools.partial(kernel, Y, X, Z, C, cuts), out_shape=plt...]
    unnamed x1, local copies, waits for them, and re-layouts: 1.88 us -> 0.8 us
where the time goes in v4:
time: 98.4 us; the launch traced here: 98.2 us
  Pallas kernels  97.4 us (99%)
    pallas_call x1, Pallas kernels, local(): pl.pallas_call(functools.partial(kernel, Y, X, Z, C, cuts), out_shape=plt...  97.4 us

profile of v4, /device:TPU:0, one launch (start us, length us, event | category | flops | bytes accessed | tf_op | source)
XLA Modules:
  0.0 98.2 jit_solution(7536122285503981606)
XLA Ops:
  0.0 97.4 %shard_map.55 = bf16[128,2048]{1,0:T(8,128)(2,1)S(1)} custom-call(bf16[128,2048]{1,0:T(8,128)(2,1)} %tok.1, f32[1,2048]{1,0:T(1,128)} %bitcast.5, bf16[704,512]{1,0:T(8,128)(2,1)} %bitcast.3, bf16[704,512]{1,0:T(8,128)(2,1)} %bitcast.4, bf16[704,512]{1,0:T(8,128)(2,1)} %dw.1), custom_call_target="tpu_custom_call" | custom-call | tf_op jit(solution)/shard_map/pallas_call | solution.py:364
  97.4 0.8 copy.7

commit v5 on v4

--- a/solution.py
+++ b/solution.py
@@ -53,9 +53,6 @@
     for cp in own_copies:
         cp.start()
 
-    values = tok[...].astype(F32)
-    factor = lax.rsqrt(jnp.mean(values * values, axis=-1, keepdims=True) + eps_floor)
-    nrm[c, z] = (values * factor * gain[...]).astype(BF16)
     pl.semaphore_wait(barrier, len(peers) + (z > 0).astype(jnp.int32) + (z < Z - 1).astype(jnp.int32))
     for cp in own_copies:
         cp.wait()
@@ -161,6 +158,9 @@
                 pl.when(ok)(cp.start)
 
     phase_one((0, 1))
+    values = tok[...].astype(F32)
+    factor = lax.rsqrt(jnp.mean(values * values, axis=-1, keepdims=True) + eps_floor)
+    nrm[c, z] = (values * factor * gain[...]).astype(BF16)
     tok_start(0)
     if C > 1:
         tok_sib(z).start()

time: 98.4 us -> 98.4 us (level)
  no operation moved by 1% of the time
where the time goes in v5:
time: 98.4 us; the launch traced here: 98.2 us
  Pallas kernels  97.4 us (99%)
    pallas_call x1, Pallas kernels, local(): pl.pallas_call(functools.partial(kernel, Y, X, Z, C, cuts), out_shape=plt...  97.4 us

profile of v5, /device:TPU:0, one launch (start us, length us, event | category | flops | bytes accessed | tf_op | source)
XLA Modules:
  0.0 98.2 jit_solution(3568475256546775424)
XLA Ops:
  0.0 97.4 %shard_map.55 = bf16[128,2048]{1,0:T(8,128)(2,1)S(1)} custom-call(bf16[128,2048]{1,0:T(8,128)(2,1)} %tok.1, f32[1,2048]{1,0:T(1,128)} %bitcast.5, bf16[704,512]{1,0:T(8,128)(2,1)} %bitcast.3, bf16[704,512]{1,0:T(8,128)(2,1)} %bitcast.4, bf16[704,512]{1,0:T(8,128)(2,1)} %dw.1), custom_call_target="tpu_custom_call" | custom-call | tf_op jit(solution)/shard_map/pallas_call | solution.py:364
  97.4 0.8 copy.7
